TPU v7x, 32 devices: a whole 2x2x4 slice. The times are simulated.
32 devices in a mesh: ep: 8 (over z, core), tp: 4 (over y, x).
Axes of the slice: x: 2, y: 2, z: 4, core: 2. Of those that a mesh axis runs over, the one named last changes fastest.
Arguments:
- tokens: bfloat16 [128, 2048], P('ep'), may hold values from -6 to 6
- old_state: float32 [128, 16, 128, 128], P('ep', 'tp'), may hold values from -2 to 2
- lower_bound: float32 [2048], P('tp'), may hold values from 0.05 to 0.95
- head_gain: float32 [2048], P('tp'), may hold values from 0.1 to 1.9
- norm_gains: float32 [4, 2048], replicated, may hold values from 0.1 to 1.9
- w_query: bfloat16 [2048, 2048], P('ep', 'tp'), may hold values from -0.125 to 0.125
- w_forget: bfloat16 [2048, 2048], P('ep', 'tp'), may hold values from -0.125 to 0.125
- w_value: bfloat16 [2048, 2048], P('ep', 'tp'), may hold values from -0.125 to 0.125
- w_outgate: bfloat16 [2048, 2048], P('ep', 'tp'), may hold values from -0.125 to 0.125
- w_mix_out: bfloat16 [2048, 2048], P('tp', 'ep'), may hold values from -0.125 to 0.125
- routes: int32 [128, 2], P('ep'), may hold values from 0 to 7, all different within a row; in each aligned block of 16 rows (0 to 15, 16 to 31, ...) at most 8 rows name the same one
- route_scores: float32 [128, 2], P('ep'), may hold values from -6 to 6
- w_exp_gate: bfloat16 [8, 2048, 3584], P('ep', None, 'tp'), may hold values from -0.125 to 0.125
- w_exp_up: bfloat16 [8, 2048, 3584], P('ep', None, 'tp'), may hold values from -0.125 to 0.125
- w_exp_down: bfloat16 [8, 3584, 2048], P('ep', 'tp'), may hold values from -0.75 to 0.75
- w_dense_gate: bfloat16 [2048, 6144], P('ep', 'tp'), may hold values from -0.125 to 0.125
- w_dense_up: bfloat16 [2048, 6144], P('ep', 'tp'), may hold values from -0.125 to 0.125
- w_dense_down: bfloat16 [6144, 2048], P('tp', 'ep'), may hold values from -0.75 to 0.75
- dense_mix: bfloat16 [2048], replicated, may hold values from -0.125 to 0.125
Outputs:
- layer_out: bfloat16 [128, 2048], P('ep', 'tp')
- new_state: float32 [128, 16, 128, 128], P('ep', 'tp')
Inputs may be any that keep to these rules, and one draw needn't show every extreme that they name: `routes`: each row names 2 different experts. In each aligned block of 16 rows no expert is named by more than 8 rows, and in every draw some expert is named by exactly 8 rows of some block.
All inputs are finite; a program needn't handle non-finite values.
Results may differ from a plain program's by a relative error of at most 0.025.
Values may be sent and summed in bfloat16 or wider, within the bound.
No kernel may reach another device: no remote copies, remote signals or barrier semaphores. Data moves between devices by JAX's collectives and lax.ppermute only.
A program may use at most 64 MiB of HBM per device.

v0:
```python
import jax
import jax.numpy as jnp
from jax import lax
from jax.sharding import PartitionSpec as P

EPS = 1e-06


def rms_scale(values):
    return lax.rsqrt(jnp.mean(values * values, axis=-1, keepdims=True) + EPS)


def body(
    tokens,
    old_state,
    lower_bound,
    head_gain,
    norm_gains,
    w_query,
    w_forget,
    w_value,
    w_outgate,
    w_mix_out,
    routes,
    route_scores,
    w_exp_gate,
    w_exp_up,
    w_exp_down,
    w_dense_gate,
    w_dense_up,
    w_dense_down,
    dense_mix,
):
    highest = lax.Precision.HIGHEST
    seqs, width = tokens.shape
    column_index = lax.axis_index("tp")
    part_width = width // lax.axis_size("tp")
    resid = tokens.astype(jnp.float32)
    normed = (resid * rms_scale(resid) * norm_gains[0]).astype(jnp.bfloat16)
    in_weights = jnp.concatenate([w_query, w_forget, w_value, w_outgate], axis=1)
    mix_rows = lax.all_to_all(normed, "ep", split_axis=1, concat_axis=0, tiled=True)
    projected = lax.psum_scatter(
        jnp.dot(mix_rows, in_weights, preferred_element_type=jnp.float32).astype(jnp.bfloat16),
        "ep",
        scatter_dimension=0,
        tiled=True,
    ).astype(jnp.float32)
    query_raw, forget_raw, value, out_gate = jnp.split(projected, 4, axis=1)
    heads = old_state.shape[1]
    head_size = old_state.shape[2]
    shape_heads = (seqs, heads, head_size)
    forget = lower_bound + (1.0 - lower_bound) * jax.nn.sigmoid(forget_raw)
    key_in = (1.0 - lower_bound) * jax.nn.sigmoid(-forget_raw)
    new_state = forget.reshape(shape_heads)[..., None] * old_state + key_in.reshape(shape_heads)[
        ..., None
    ] * value.reshape(seqs, heads, 1, head_size)
    query = jax.nn.silu(query_raw).reshape(shape_heads)
    read = jnp.einsum("thk,thkv->thv", query, new_state, precision=highest)
    gated = (
        read
        * rms_scale(read)
        * head_gain.reshape(heads, head_size)
        * jax.nn.silu(out_gate).reshape(shape_heads)
    )
    mixed_heads = gated.reshape(seqs, heads * head_size).astype(jnp.bfloat16)
    mix_part = jnp.dot(
        mixed_heads,
        lax.all_gather(w_mix_out, "ep", axis=1, tiled=True),
        preferred_element_type=jnp.float32,
    ).astype(jnp.bfloat16)
    mix_part = lax.optimization_barrier(mix_part).astype(jnp.float32)
    mix_out = lax.psum(mix_part.astype(jnp.bfloat16), "tp")
    mix_wide = lax.optimization_barrier(mix_out).astype(jnp.float32)
    after_mix = resid + mix_wide * rms_scale(mix_wide) * norm_gains[1]
    ffn_in = (after_mix * rms_scale(after_mix) * norm_gains[2]).astype(jnp.bfloat16)
    experts = lax.axis_size("ep")
    topk = routes.shape[1]
    capacity = max(2, 2 * seqs * topk // experts)
    flat_routes = routes.reshape(-1)
    onehot = (flat_routes[:, None] == jnp.arange(experts, dtype=jnp.int32)[None, :]).astype(
        jnp.int32
    )
    before = jnp.cumsum(onehot, axis=0) - onehot
    slots = jnp.sum(onehot * before, axis=1)
    cells = flat_routes * capacity + slots
    placed = cells[None, :] == jnp.arange(experts * capacity, dtype=jnp.int32)[:, None]
    repeated = jnp.repeat(ffn_in, topk, axis=0)
    outgoing = jnp.dot(placed.astype(jnp.bfloat16), repeated, preferred_element_type=jnp.float32)
    outgoing = outgoing.astype(jnp.bfloat16).reshape(experts, capacity, width)
    arrived = lax.all_to_all(outgoing, "ep", split_axis=0, concat_axis=0, tiled=True)
    sources, items, _ = arrived.shape
    expert_rows = arrived.reshape(sources * items, width)
    gate_pre = jnp.dot(expert_rows, w_exp_gate[0], preferred_element_type=jnp.float32)
    up_pre = jnp.dot(expert_rows, w_exp_up[0], preferred_element_type=jnp.float32)
    hidden = (jax.nn.silu(gate_pre) * up_pre).astype(jnp.bfloat16)
    partial_rows = jnp.dot(hidden, w_exp_down[0], preferred_element_type=jnp.float32).astype(
        jnp.bfloat16
    )
    partial_rows = lax.optimization_barrier(partial_rows).astype(jnp.float32)
    partial_rows = partial_rows.reshape(sources, items, width)
    summed = lax.psum_scatter(
        partial_rows.astype(jnp.bfloat16), "tp", scatter_dimension=2, tiled=True
    )
    returned = lax.all_to_all(summed, "ep", split_axis=0, concat_axis=0, tiled=True)
    first = jax.nn.sigmoid(route_scores[:, 0] - route_scores[:, 1])
    second = jax.nn.sigmoid(route_scores[:, 1] - route_scores[:, 0])
    route_weight = jnp.stack([first, second], axis=1).reshape(-1)
    weight_table = jnp.sum(
        (placed.astype(jnp.float32) * route_weight[None, :]).reshape(
            experts * capacity, seqs, topk
        ),
        axis=2,
    )
    expert_sum = jnp.dot(
        weight_table.T,
        returned.reshape(experts * capacity, part_width).astype(jnp.float32),
        precision=highest,
    )
    dense_weights = jnp.concatenate([w_dense_gate, w_dense_up], axis=1)
    dense_rows = lax.all_to_all(ffn_in, "ep", split_axis=1, concat_axis=0, tiled=True)
    dense_pre = lax.psum_scatter(
        jnp.dot(dense_rows, dense_weights, preferred_element_type=jnp.float32).astype(jnp.bfloat16),
        "ep",
        scatter_dimension=0,
        tiled=True,
    ).astype(jnp.float32)
    dense_gate_pre, dense_up_pre = jnp.split(dense_pre, 2, axis=1)
    dense_hidden = (jax.nn.silu(dense_gate_pre) * dense_up_pre).astype(jnp.bfloat16)
    dense_partial = jnp.dot(
        dense_hidden,
        lax.all_gather(w_dense_down, "ep", axis=1, tiled=True),
        preferred_element_type=jnp.float32,
    )
    dense_out = lax.psum_scatter(
        dense_partial.astype(jnp.bfloat16), "tp", scatter_dimension=1, tiled=True
    ).astype(jnp.float32)
    mix_weight = jax.nn.sigmoid(jnp.dot(ffn_in, dense_mix, preferred_element_type=jnp.float32))
    ffn_out = expert_sum + mix_weight[:, None] * dense_out
    squares = lax.psum(jnp.sum(ffn_out * ffn_out, axis=1), "tp")
    out_scale = lax.rsqrt(squares / width + EPS)
    gain_part = lax.dynamic_slice_in_dim(norm_gains[3], column_index * part_width, part_width, 0)
    resid_part = lax.dynamic_slice_in_dim(after_mix, column_index * part_width, part_width, 1)
    layer_out = (resid_part + ffn_out * out_scale[:, None] * gain_part).astype(jnp.bfloat16)
    return (layer_out, new_state)


def solution(mesh):
    return jax.shard_map(
        body,
        mesh=mesh,
        in_specs=(
            P("ep", None),
            P("ep", "tp", None, None),
            P("tp"),
            P("tp"),
            P(),
            P("ep", "tp"),
            P("ep", "tp"),
            P("ep", "tp"),
            P("ep", "tp"),
            P("tp", "ep"),
            P("ep", None),
            P("ep", None),
            P("ep", None, "tp"),
            P("ep", None, "tp"),
            P("ep", "tp", None),
            P("ep", "tp"),
            P("ep", "tp"),
            P("tp", "ep"),
            P(),
        ),
        out_specs=(P("ep", "tp"), P("ep", "tp", None, None)),
        check_vma=False,
    )
```

profile of v0, /device:TPU:0, one launch (start us, length us, event | category | flops | bytes accessed | tf_op | source)
XLA Modules:
  0.0 319.4 jit_solution(3477213161517081613)
XLA Ops:
  7.2 0.9 fusion.58
  8.2 1.0 fusion.42
  9.2 0.9 fusion.44
  10.1 12.1 %all_to_all.48 = bf16[16,8,256]{2,0,1:T(8,128)(2,1)S(1)} all-to-all(bf16[16,8,256]{2,0,1:T(8,128)(2,1)S(1)} %bitcast.82), channel_id=1, replica_groups=mesh['ep'=8,'tp'=4] {'ep'}, dimensions={1} | all-to-all | bytes 131072 | tf_op jit(solution)/shard_map/all_to_all | solution.py:41
  22.2 2.3 convolution_convert_fusion.1
  24.5 0.7 all-gather.3.cloned.1.call-update
  25.8 28.7 %reduce-scatter.5.cloned.1.call-done = bf16[16,2048]{1,0:T(8,128)(2,1)} async-done(((bf16[128,2048]{1,0:T(8,128)(2,1)}), bf16[16,2048]{1,0:T(8,128)(2,1)}) %reduce-scatter.5.cloned.1.call-update) | async-done | bytes 65552 | tf_op jit(solution)/shard_map/reduce_scatter | solution.py:42
  54.5 0.8 convert_element_type.70
  55.4 0.7 split.26
  56.2 4.4 %multiply_add_fusion = f32[16,4,128,128]{3,2,1,0:T(8,128)S(1)} fusion(f32[16,4,128,128]{3,2,1,0:T(8,128)} %param.20, f32[16,4,128]{2,1,0:T(4,128)S(1)} %mul.223, f32[16,4,128]{2,1,0:T(4,128)S(1)} %mul.221, f32[16,4,128]{2,1,0:T(4,128)S(1)} %mul.217), kind=kLoop, calls=%fused_computation | loop fusion | flops 3145728 | bytes 8486912 | tf_op jit(solution)/shard_map/add | solution.py:54
  60.7 2.0 copy-done
  62.6 3.7 %fusion.59 = f32[16,4,1,128]{3,2,1,0:T(1,128)S(1)} fusion(f32[16,4,128,1]{2,3,1,0:T(1,128)S(1)} %bitcast.84, f32[16,4,128,128]{3,2,1,0:T(8,128)S(1)} %multiply_add_fusion), kind=kOutput, calls=%fused_computation.92 | convolution fusion | flops 12582912 | bytes 4259840 | tf_op jit(solution)/shard_map/thk,thkv->thv/dot_general | solution.py:58
  66.5 18.5 %all-gather.3.cloned.1.call-done = bf16[512,2048]{1,0:T(8,128)(2,1)} async-done(((bf16[512,256]{1,0:T(8,128)(2,1)}), bf16[512,2048]{1,0:T(8,128)(2,1)}) %all-gather.3.cloned.1.call-update) | async-done | bytes 2097168 | tf_op jit(solution)/shard_map/all_gather | solution.py:68
  85.0 2.6 convolution_convert_fusion.4
  87.7 41.1 %all-reduce.2.cloned.1.call-done = bf16[16,2048]{1,0:T(8,128)(2,1)} async-done(((bf16[16,2048]{1,0:T(8,128)(2,1)}), bf16[16,2048]{1,0:T(8,128)(2,1)}) %all-reduce.2.cloned.1.call-update) | async-done | bytes 65552 | tf_op jit(solution)/shard_map/psum | solution.py:72
  128.8 1.0 fusion.40
  129.7 1.0 multiply_reduce_fusion
  131.2 14.1 %all_to_all.49 = bf16[8,8,2048]{2,1,0:T(8,128)(2,1)S(1)} all-to-all(bf16[8,8,2048]{2,1,0:T(8,128)(2,1)S(1)} %fusion.9), channel_id=1, replica_groups=mesh['ep'=8,'tp'=4] {'ep'}, dimensions={0} | all-to-all | bytes 524288 | tf_op jit(solution)/shard_map/all_to_all | solution.py:90
  145.4 2.7 fusion.4
  148.1 5.5 %fusion.6 = bf16[64,2048]{1,0:T(8,128)(2,1)} fusion(bf16[1,896,2048]{2,1,0:T(8,128)(2,1)} %param.33, bf16[1,2048,896]{2,1,0:T(8,128)(2,1)} %param.32, bf16[8,8,2048]{2,1,0:T(8,128)(2,1)S(1)} %all_to_all.49, f32[64,896]{1,0:T(8,128)S(1)} %fusion.4), kind=kOutput, calls=%fused_computation.9 | convolution fusion | flops 470237184 | bytes 8093696 | tf_op jit(solution)/shard_map/dot_general | solution.py:96
  153.7 8.3 %all_to_all.50 = bf16[16,8,256]{2,0,1:T(8,128)(2,1)S(1)} all-to-all(bf16[16,8,256]{2,0,1:T(8,128)(2,1)S(1)} %bitcast.83), channel_id=1, replica_groups=mesh['ep'=8,'tp'=4] {'ep'}, dimensions={1} | all-to-all | bytes 131072 | tf_op jit(solution)/shard_map/all_to_all | solution.py:120
  162.0 1.3 convolution_convert_fusion
  164.2 11.9 %reduce-scatter.7.cloned.1.call-done = bf16[8,8,512]{2,1,0:T(8,128)(2,1)} async-done(((bf16[8,8,2048]{2,1,0:T(8,128)(2,1)}), bf16[8,8,512]{2,1,0:T(8,128)(2,1)}) %reduce-scatter.7.cloned.1.call-update) | async-done | bytes 65552 | tf_op jit(solution)/shard_map/reduce_scatter | solution.py:101
  176.1 4.6 %all-to-all-start.2 = ((bf16[8,8,512]{2,1,0:T(8,128)(2,1)}), bf16[8,8,512]{2,1,0:T(8,128)(2,1)S(1)}, u32[]{:S(2)}, u32[]{:S(2)}) async-start(bf16[8,8,512]{2,1,0:T(8,128)(2,1)} %reduce-scatter.7.cloned.1.call-done), calls=%async_computation.4 | async-start | bytes 131072 | tf_op jit(solution)/shard_map/all_to_all | solution.py:104
  180.8 29.5 %reduce-scatter.9.cloned.1.call-done = bf16[16,3072]{1,0:T(8,128)(2,1)} async-done(((bf16[128,3072]{1,0:T(8,128)(2,1)}), bf16[16,3072]{1,0:T(8,128)(2,1)}) %reduce-scatter.9.cloned.1.call-update) | async-done | bytes 98320 | tf_op jit(solution)/shard_map/reduce_scatter | solution.py:121
  210.3 0.9 convert_element_type.82
  211.2 63.9 %all-gather.5.cloned.1.call-done = bf16[1536,2048]{1,0:T(8,128)(2,1)} async-done(((bf16[1536,256]{1,0:T(8,128)(2,1)}), bf16[1536,2048]{1,0:T(8,128)(2,1)}) %all-gather.5.cloned.1.call-update) | async-done | bytes 6291472 | tf_op jit(solution)/shard_map/all_gather | solution.py:131
  275.1 4.3 %convolution_convert_fusion.3 = bf16[16,2048]{1,0:T(8,128)(2,1)} fusion(bf16[1536,2048]{1,0:T(8,128)(2,1)} %all-gather.5.cloned.1.call-done, f32[16,3072]{1,0:T(8,128)S(1)} %convert_element_type.82), kind=kOutput, calls=%fused_computation.12 | convolution fusion | flops 100843520 | bytes 6553600 | tf_op jit(solution)/shard_map/dot_general | solution.py:129
  279.6 22.3 %reduce-scatter.11.cloned.1.call-done = bf16[16,512]{1,0:T(8,128)(2,1)} async-done(((bf16[16,2048]{1,0:T(8,128)(2,1)}), bf16[16,512]{1,0:T(8,128)(2,1)}) %reduce-scatter.11.cloned.1.call-update) | async-done | bytes 16400 | tf_op jit(solution)/shard_map/reduce_scatter | solution.py:134
  301.9 1.0 multiply_reduce_fusion.1
  302.9 8.9 %psum.15 = f32[16]{0:T(128)S(1)} all-reduce(f32[16]{0:T(128)S(1)} %get-tuple-element.14), channel_id=1, replica_groups=mesh['ep'=8,'tp'=4] {'tp'}, use_global_device_ids=true, to_apply=%region_13.14 | all-reduce | flops 16 | bytes 128 | tf_op jit(solution)/shard_map/psum | solution.py:139
  311.8 0.7 add_convert_fusion
  (66 shorter events, 2.6 us)
Async XLA Ops:
  7.2 18.1 %copy-start.4 = (s32[16,2]{0,1:T(2,128)S(1)}, s32[16,2]{0,1:T(2,128)}, u32[]{:S(2)}) copy-start(s32[16,2]{0,1:T(2,128)} %param.29) | copy-start | bytes 388
  7.2 18.6 %copy-start.2 = (f32[512]{0:T(512)S(1)}, f32[512]{0:T(512)}, u32[]{:S(2)}) copy-start(f32[512]{0:T(512)} %param.21) | copy-start | bytes 6148
  7.2 47.3 %reduce-scatter.5.cloned.1.call-start = ((), (), s32[]{:S(2)}) async-start(), calls=%async_computation.8 | async-start | bytes 589824 | tf_op jit(solution)/shard_map/reduce_scatter | solution.py:42
  24.5 60.5 %all-gather.3.cloned.1.call-start = ((), (), s32[]{:S(2)}) async-start(), calls=%async_computation.9 | async-start | bytes 2359296 | tf_op jit(solution)/shard_map/all_gather | solution.py:68
  25.2 103.5 %all-reduce.2.cloned.1.call-start = ((), (), s32[]{:S(2)}) async-start(), calls=%async_computation.10 | async-start | bytes 131072 | tf_op jit(solution)/shard_map/psum | solution.py:72
  60.6 2.0 copy-start
  60.6 5.8 %copy-start.5 = (f32[512]{0:T(512)S(1)}, f32[512]{0:T(512)}, u32[]{:S(2)}) copy-start(f32[512]{0:T(512)} %param.22) | copy-start | bytes 6148
  60.6 69.1 %copy-start.1 = (bf16[16,2048]{1,0:T(8,128)(2,1)S(1)}, bf16[16,2048]{1,0:T(8,128)(2,1)}, u32[]{:S(2)}) copy-start(bf16[16,2048]{1,0:T(8,128)(2,1)} %param.19) | copy-start | bytes 196612
  87.6 88.5 %reduce-scatter.7.cloned.1.call-start = ((), (), s32[]{:S(2)}) async-start(), calls=%async_computation.11 | async-start | bytes 327680 | tf_op jit(solution)/shard_map/reduce_scatter | solution.py:101
  148.1 13.9 %copy-start.7 = (bf16[256,1536]{1,0:T(8,128)(2,1)S(1)}, bf16[256,1536]{1,0:T(8,128)(2,1)}, u32[]{:S(2)}) copy-start(bf16[256,1536]{1,0:T(8,128)(2,1)} %param.35) | copy-start | bytes 2359300
  148.1 13.9 %copy-start.8 = (bf16[256,1536]{1,0:T(8,128)(2,1)S(1)}, bf16[256,1536]{1,0:T(8,128)(2,1)}, u32[]{:S(2)}) copy-start(bf16[256,1536]{1,0:T(8,128)(2,1)} %param.34) | copy-start | bytes 2359300
  153.6 10.3 %copy-start.3 = (bf16[2048]{0:T(1024)(128)(2,1)S(1)}, bf16[2048]{0:T(1024)(128)(2,1)}, u32[]{:S(2)}) copy-start(bf16[2048]{0:T(1024)(128)(2,1)} %param.37) | copy-start | bytes 12292
  153.6 10.5 %copy-start.6 = (f32[16,2]{0,1:T(2,128)S(1)}, f32[16,2]{0,1:T(2,128)}, u32[]{:S(2)}) copy-start(f32[16,2]{0,1:T(2,128)} %param.30) | copy-start | bytes 388
  153.7 56.6 %reduce-scatter.9.cloned.1.call-start = ((), (), s32[]{:S(2)}) async-start(), calls=%async_computation.12 | async-start | bytes 884736 | tf_op jit(solution)/shard_map/reduce_scatter | solution.py:121
  163.3 111.8 %all-gather.5.cloned.1.call-start = ((), (), s32[]{:S(2)}) async-start(), calls=%async_computation.13 | async-start | bytes 7077888 | tf_op jit(solution)/shard_map/all_gather | solution.py:131
  176.1 103.5 %all-to-all-start.2 = ((bf16[8,8,512]{2,1,0:T(8,128)(2,1)}), bf16[8,8,512]{2,1,0:T(8,128)(2,1)S(1)}, u32[]{:S(2)}, u32[]{:S(2)}) async-start(bf16[8,8,512]{2,1,0:T(8,128)(2,1)} %reduce-scatter.7.cloned.1.call-done), calls=%async_computation.4 | async-start | bytes 131072 | tf_op jit(solution)/shard_map/all_to_all | solution.py:104
  180.7 121.2 %reduce-scatter.11.cloned.1.call-start = ((), (), s32[]{:S(2)}) async-start(), calls=%async_computation.14 | async-start | bytes 81920 | tf_op jit(solution)/shard_map/reduce_scatter | solution.py:134
Sparse Core Ops, SparseCore 0:
  24.6 29.8 reduce-scatter.4
  56.1 28.8 all-gather.2
  87.9 40.8 all-reduce.1
  153.8 22.2 reduce-scatter.6
  178.2 31.9 reduce-scatter.8
  211.7 63.3 all-gather.4
  279.6 22.2 reduce-scatter.10
where the time goes:
time: 320 us; the launch traced here: 319 us
  waiting for transfers between devices  217 us (68%)
  blocking collectives  43.4 us (14%)
  matrix products  23.7 us (7%)
  between operations  14.4 us (4%)
  other arithmetic  11.5 us (4%)
  starting transfers between devices  4.89 us (2%)
  local copies, waits for them, and re-layouts  4.25 us (1%)
    all_gather x1, waiting for transfers between devices, body(): lax.all_gather(w_dense_down, 'ep', axis=1, tiled=True)  63.9 us
    psum x1, waiting for transfers between devices, body(): mix_out = lax.psum(mix_part.astype(jnp.bfloat16), 'tp')  41.1 us
    reduce_scatter x1, waiting for transfers between devices, body(): lax.psum_scatter(jnp.dot(dense_rows, dense_weights, preferred_element_typ...  29.5 us
    reduce_scatter x1, waiting for transfers between devices, body(): lax.psum_scatter(jnp.dot(mix_rows, in_weights, preferred_element_type=jnp...  28.7 us
    reduce_scatter x1, waiting for transfers between devices, body(): lax.psum_scatter(dense_partial.astype(jnp.bfloat16), 'tp', scatter_dimens...  22.3 us
    all_gather x1, waiting for transfers between devices, body(): lax.all_gather(w_mix_out, 'ep', axis=1, tiled=True)  18.5 us
    all_to_all x1, blocking collectives, body(): lax.all_to_all(outgoing, 'ep', split_axis=0, concat_axis=0, tiled=True)  14.1 us
    all_to_all x1, blocking collectives, body(): lax.all_to_all(normed, 'ep', split_axis=1, concat_axis=0, tiled=True)  12.1 us
  transfers between devices with their start and end apart: 8, of which 7 were waited for; matrix products, arithmetic and copies ran while one was open for 5% of the time, Pallas kernels for 0%

commit v1 on v0

--- a/solution.py
+++ b/solution.py
@@ -69,7 +69,7 @@
         preferred_element_type=jnp.float32,
     ).astype(jnp.bfloat16)
     mix_part = lax.optimization_barrier(mix_part).astype(jnp.float32)
-    mix_out = lax.psum(mix_part.astype(jnp.bfloat16), "tp")
+    mix_out = jnp.sum(lax.all_gather(mix_part.astype(jnp.bfloat16), "tp"), axis=0)
     mix_wide = lax.optimization_barrier(mix_out).astype(jnp.float32)
     after_mix = resid + mix_wide * rms_scale(mix_wide) * norm_gains[1]
     ffn_in = (after_mix * rms_scale(after_mix) * norm_gains[2]).astype(jnp.bfloat16)

time: 320 us -> 285 us (0.89)
  waiting for transfers between devices: 217 us -> 177 us
  blocking collectives: 43.4 us -> 50.8 us
    psum x1 -> x0, waiting for transfers between devices: 41.1 us -> none  [body(): mix_out = lax.psum(mix_part.astype(jnp.bfloat16), 'tp')]
    all_gather x0 -> x1, blocking collectives: none -> 8.87 us  [body(): lax.all_gather(mix_part.astype(jnp.bfloat16), 'tp')]
  transfers between devices with their start and end apart: 8 -> 7, of which waited for: 7 -> 6; matrix products, arithmetic and copies ran while one was open for 5% -> 6% of each run, Pallas kernels for 0% -> 0%
where the time goes in v1:
time: 285 us; the launch traced here: 284 us
  waiting for transfers between devices  177 us (62%)
  blocking collectives  50.8 us (18%)
  matrix products  23.1 us (8%)
  between operations  14.4 us (5%)
  other arithmetic  9.89 us (3%)
  starting transfers between devices  4.83 us (2%)
  local copies, waits for them, and re-layouts  4.25 us (1%)
    all_gather x1, waiting for transfers between devices, body(): lax.all_gather(w_dense_down, 'ep', axis=1, tiled=True)  64.1 us
    reduce_scatter x1, waiting for transfers between devices, body(): lax.psum_scatter(jnp.dot(dense_rows, dense_weights, preferred_element_typ...  29.4 us
    reduce_scatter x1, waiting for transfers between devices, body(): lax.psum_scatter(jnp.dot(mix_rows, in_weights, preferred_element_type=jnp...  28.7 us
    reduce_scatter x1, waiting for transfers between devices, body(): lax.psum_scatter(dense_partial.astype(jnp.bfloat16), 'tp', scatter_dimens...  22.3 us
    all_gather x1, waiting for transfers between devices, body(): lax.all_gather(w_mix_out, 'ep', axis=1, tiled=True)  18.4 us
    all_to_all x1, blocking collectives, body(): lax.all_to_all(outgoing, 'ep', split_axis=0, concat_axis=0, tiled=True)  12.6 us
    reduce_scatter x1, waiting for transfers between devices, body(): lax.psum_scatter(partial_rows.astype(jnp.bfloat16), 'tp', scatter_dimensi...  12.5 us
    all_to_all x1, blocking collectives, body(): lax.all_to_all(normed, 'ep', split_axis=1, concat_axis=0, tiled=True)  12.1 us
  transfers between devices with their start and end apart: 7, of which 6 were waited for; matrix products, arithmetic and copies ran while one was open for 6% of the time, Pallas kernels for 0%

profile of v1, /device:TPU:0, one launch (start us, length us, event | category | flops | bytes accessed | tf_op | source)
XLA Modules:
  0.0 283.9 jit_solution(10849067463388183887)
XLA Ops:
  7.2 0.9 fusion.58
  8.2 1.0 fusion.42
  9.2 0.9 fusion.44
  10.1 12.1 %all_to_all.48 = bf16[16,8,256]{2,0,1:T(8,128)(2,1)S(1)} all-to-all(bf16[16,8,256]{2,0,1:T(8,128)(2,1)S(1)} %bitcast.84), channel_id=1, replica_groups=mesh['ep'=8,'tp'=4] {'ep'}, dimensions={1} | all-to-all | bytes 131072 | tf_op jit(solution)/shard_map/all_to_all | solution.py:41
  22.2 2.3 convolution_convert_fusion.1
  24.5 0.7 all-gather.4.cloned.1.call-update
  25.8 28.7 %reduce-scatter.5.cloned.1.call-done = bf16[16,2048]{1,0:T(8,128)(2,1)} async-done(((bf16[128,2048]{1,0:T(8,128)(2,1)}), bf16[16,2048]{1,0:T(8,128)(2,1)}) %reduce-scatter.5.cloned.1.call-update) | async-done | bytes 65552 | tf_op jit(solution)/shard_map/reduce_scatter | solution.py:42
  54.5 0.8 convert_element_type.72
  55.4 0.7 split.26
  56.2 4.4 %multiply_add_fusion = f32[16,4,128,128]{3,2,1,0:T(8,128)S(1)} fusion(f32[16,4,128,128]{3,2,1,0:T(8,128)} %param.20, f32[16,4,128]{2,1,0:T(4,128)S(1)} %mul.223, f32[16,4,128]{2,1,0:T(4,128)S(1)} %mul.221, f32[16,4,128]{2,1,0:T(4,128)S(1)} %mul.217), kind=kLoop, calls=%fused_computation | loop fusion | flops 3145728 | bytes 8486912 | tf_op jit(solution)/shard_map/add | solution.py:54
  60.6 2.0 copy-done
  62.6 3.7 %fusion.59 = f32[16,4,1,128]{3,2,1,0:T(1,128)S(1)} fusion(f32[16,4,128,1]{2,3,1,0:T(1,128)S(1)} %bitcast.86, f32[16,4,128,128]{3,2,1,0:T(8,128)S(1)} %multiply_add_fusion), kind=kOutput, calls=%fused_computation.92 | convolution fusion | flops 12582912 | bytes 4259840 | tf_op jit(solution)/shard_map/thk,thkv->thv/dot_general | solution.py:58
  66.5 18.4 %all-gather.4.cloned.1.call-done = bf16[512,2048]{1,0:T(8,128)(2,1)} async-done(((bf16[512,256]{1,0:T(8,128)(2,1)}), bf16[512,2048]{1,0:T(8,128)(2,1)}) %all-gather.4.cloned.1.call-update) | async-done | bytes 2097168 | tf_op jit(solution)/shard_map/all_gather | solution.py:68
  84.9 2.0 convolution_convert_fusion.4
  86.9 8.9 %all-gather = bf16[64,2048]{1,0:T(8,128)(2,1)S(1)} all-gather(bf16[16,2048]{1,0:T(8,128)(2,1)S(1)} %convolution_convert_fusion.4), channel_id=2, replica_groups=mesh['ep'=8,'tp'=4] {'tp'}, dimensions={0}, use_global_device_ids=true | all-gather | bytes 327680 | tf_op jit(solution)/shard_map/all_gather | solution.py:72
  95.9 0.2 multiply_reduce_fusion
  96.6 12.6 %all_to_all.49 = bf16[8,8,2048]{2,1,0:T(8,128)(2,1)S(1)} all-to-all(bf16[8,8,2048]{2,1,0:T(8,128)(2,1)S(1)} %fusion.9), channel_id=1, replica_groups=mesh['ep'=8,'tp'=4] {'ep'}, dimensions={0} | all-to-all | bytes 524288 | tf_op jit(solution)/shard_map/all_to_all | solution.py:90
  109.2 2.7 fusion.4
  112.0 5.5 %fusion.6 = bf16[64,2048]{1,0:T(8,128)(2,1)} fusion(bf16[1,896,2048]{2,1,0:T(8,128)(2,1)} %param.33, bf16[1,2048,896]{2,1,0:T(8,128)(2,1)} %param.32, bf16[8,8,2048]{2,1,0:T(8,128)(2,1)S(1)} %all_to_all.49, f32[64,896]{1,0:T(8,128)S(1)} %fusion.4), kind=kOutput, calls=%fused_computation.9 | convolution fusion | flops 470237184 | bytes 8093696 | tf_op jit(solution)/shard_map/dot_general | solution.py:96
  117.6 8.3 %all_to_all.50 = bf16[16,8,256]{2,0,1:T(8,128)(2,1)S(1)} all-to-all(bf16[16,8,256]{2,0,1:T(8,128)(2,1)S(1)} %bitcast.85), channel_id=1, replica_groups=mesh['ep'=8,'tp'=4] {'ep'}, dimensions={1} | all-to-all | bytes 131072 | tf_op jit(solution)/shard_map/all_to_all | solution.py:120
  125.9 1.3 convolution_convert_fusion
  127.2 0.5 all-gather.6.cloned.1.call-update
  128.1 12.5 %reduce-scatter.7.cloned.1.call-done = bf16[8,8,512]{2,1,0:T(8,128)(2,1)} async-done(((bf16[8,8,2048]{2,1,0:T(8,128)(2,1)}), bf16[8,8,512]{2,1,0:T(8,128)(2,1)}) %reduce-scatter.7.cloned.1.call-update) | async-done | bytes 65552 | tf_op jit(solution)/shard_map/reduce_scatter | solution.py:101
  140.6 4.6 %all-to-all-start.2 = ((bf16[8,8,512]{2,1,0:T(8,128)(2,1)}), bf16[8,8,512]{2,1,0:T(8,128)(2,1)S(1)}, u32[]{:S(2)}, u32[]{:S(2)}) async-start(bf16[8,8,512]{2,1,0:T(8,128)(2,1)} %reduce-scatter.7.cloned.1.call-done), calls=%async_computation.4 | async-start | bytes 131072 | tf_op jit(solution)/shard_map/all_to_all | solution.py:104
  145.2 29.4 %reduce-scatter.9.cloned.1.call-done = bf16[16,3072]{1,0:T(8,128)(2,1)} async-done(((bf16[128,3072]{1,0:T(8,128)(2,1)}), bf16[16,3072]{1,0:T(8,128)(2,1)}) %reduce-scatter.9.cloned.1.call-update) | async-done | bytes 98320 | tf_op jit(solution)/shard_map/reduce_scatter | solution.py:121
  174.6 0.9 convert_element_type.84
  175.5 64.1 %all-gather.6.cloned.1.call-done = bf16[1536,2048]{1,0:T(8,128)(2,1)} async-done(((bf16[1536,256]{1,0:T(8,128)(2,1)}), bf16[1536,2048]{1,0:T(8,128)(2,1)}) %all-gather.6.cloned.1.call-update) | async-done | bytes 6291472 | tf_op jit(solution)/shard_map/all_gather | solution.py:131
  239.6 4.3 %convolution_convert_fusion.3 = bf16[16,2048]{1,0:T(8,128)(2,1)} fusion(bf16[1536,2048]{1,0:T(8,128)(2,1)} %all-gather.6.cloned.1.call-done, f32[16,3072]{1,0:T(8,128)S(1)} %convert_element_type.84), kind=kOutput, calls=%fused_computation.12 | convolution fusion | flops 100843520 | bytes 6553600 | tf_op jit(solution)/shard_map/dot_general | solution.py:129
  244.1 22.3 %reduce-scatter.11.cloned.1.call-done = bf16[16,512]{1,0:T(8,128)(2,1)} async-done(((bf16[16,2048]{1,0:T(8,128)(2,1)}), bf16[16,512]{1,0:T(8,128)(2,1)}) %reduce-scatter.11.cloned.1.call-update) | async-done | bytes 16400 | tf_op jit(solution)/shard_map/reduce_scatter | solution.py:134
  266.4 1.0 multiply_reduce_fusion.1
  267.4 8.9 %psum.7 = f32[16]{0:T(128)S(1)} all-reduce(f32[16]{0:T(128)S(1)} %get-tuple-element.14), channel_id=1, replica_groups=mesh['ep'=8,'tp'=4] {'tp'}, use_global_device_ids=true, to_apply=%region_13.14 | all-reduce | flops 16 | bytes 128 | tf_op jit(solution)/shard_map/psum | solution.py:139
  276.3 0.7 add_convert_fusion
  (65 shorter events, 2.2 us)
Async XLA Ops:
  7.2 18.1 %copy-start.4 = (s32[16,2]{0,1:T(2,128)S(1)}, s32[16,2]{0,1:T(2,128)}, u32[]{:S(2)}) copy-start(s32[16,2]{0,1:T(2,128)} %param.29) | copy-start | bytes 388
  7.2 18.6 %copy-start.2 = (f32[512]{0:T(512)S(1)}, f32[512]{0:T(512)}, u32[]{:S(2)}) copy-start(f32[512]{0:T(512)} %param.21) | copy-start | bytes 6148
  7.2 47.3 %reduce-scatter.5.cloned.1.call-start = ((), (), s32[]{:S(2)}) async-start(), calls=%async_computation.8 | async-start | bytes 589824 | tf_op jit(solution)/shard_map/reduce_scatter | solution.py:42
  24.5 60.4 %all-gather.4.cloned.1.call-start = ((), (), s32[]{:S(2)}) async-start(), calls=%async_computation.9 | async-start | bytes 2359296 | tf_op jit(solution)/shard_map/all_gather | solution.py:68
  25.2 115.3 %reduce-scatter.7.cloned.1.call-start = ((), (), s32[]{:S(2)}) async-start(), calls=%async_computation.10 | async-start | bytes 327680 | tf_op jit(solution)/shard_map/reduce_scatter | solution.py:101
  60.6 2.0 copy-start
  60.6 5.8 %copy-start.5 = (f32[512]{0:T(512)S(1)}, f32[512]{0:T(512)}, u32[]{:S(2)}) copy-start(f32[512]{0:T(512)} %param.22) | copy-start | bytes 6148
  60.6 35.3 %copy-start.1 = (bf16[16,2048]{1,0:T(8,128)(2,1)S(1)}, bf16[16,2048]{1,0:T(8,128)(2,1)}, u32[]{:S(2)}) copy-start(bf16[16,2048]{1,0:T(8,128)(2,1)} %param.19) | copy-start | bytes 196612
  111.9 13.9 %copy-start.7 = (bf16[256,1536]{1,0:T(8,128)(2,1)S(1)}, bf16[256,1536]{1,0:T(8,128)(2,1)}, u32[]{:S(2)}) copy-start(bf16[256,1536]{1,0:T(8,128)(2,1)} %param.35) | copy-start | bytes 2359300
  112.0 13.9 %copy-start.8 = (bf16[256,1536]{1,0:T(8,128)(2,1)S(1)}, bf16[256,1536]{1,0:T(8,128)(2,1)}, u32[]{:S(2)}) copy-start(bf16[256,1536]{1,0:T(8,128)(2,1)} %param.34) | copy-start | bytes 2359300
  117.5 10.4 %copy-start.3 = (bf16[2048]{0:T(1024)(128)(2,1)S(1)}, bf16[2048]{0:T(1024)(128)(2,1)}, u32[]{:S(2)}) copy-start(bf16[2048]{0:T(1024)(128)(2,1)} %param.37) | copy-start | bytes 12292
  117.5 10.5 %copy-start.6 = (f32[16,2]{0,1:T(2,128)S(1)}, f32[16,2]{0,1:T(2,128)}, u32[]{:S(2)}) copy-start(f32[16,2]{0,1:T(2,128)} %param.30) | copy-start | bytes 388
  117.5 57.1 %reduce-scatter.9.cloned.1.call-start = ((), (), s32[]{:S(2)}) async-start(), calls=%async_computation.11 | async-start | bytes 884736 | tf_op jit(solution)/shard_map/reduce_scatter | solution.py:121
  127.2 112.4 %all-gather.6.cloned.1.call-start = ((), (), s32[]{:S(2)}) async-start(), calls=%async_computation.12 | async-start | bytes 7077888 | tf_op jit(solution)/shard_map/all_gather | solution.py:131
  140.6 103.5 %all-to-all-start.2 = ((bf16[8,8,512]{2,1,0:T(8,128)(2,1)}), bf16[8,8,512]{2,1,0:T(8,128)(2,1)S(1)}, u32[]{:S(2)}, u32[]{:S(2)}) async-start(bf16[8,8,512]{2,1,0:T(8,128)(2,1)} %reduce-scatter.7.cloned.1.call-done), calls=%async_computation.4 | async-start | bytes 131072 | tf_op jit(solution)/shard_map/all_to_all | solution.py:104
  145.2 121.2 %reduce-scatter.11.cloned.1.call-start = ((), (), s32[]{:S(2)}) async-start(), calls=%async_computation.13 | async-start | bytes 81920 | tf_op jit(solution)/shard_map/reduce_scatter | solution.py:134
Sparse Core Ops, SparseCore 0:
  24.6 29.8 reduce-scatter.4
  56.1 28.7 all-gather.3
  117.6 22.8 reduce-scatter.6
  142.7 31.8 reduce-scatter.8
  176.0 63.5 all-gather.5
  244.1 22.2 reduce-scatter.10
